TPU v7x, 256 devices: a whole 4x4x8 slice. The times are simulated.
256 devices in a mesh: ep: 64 (over z, x, core), tp: 4 (over y).
Axes of the slice: x: 4, y: 4, z: 8, core: 2. Of those that a mesh axis runs over, the one named last changes fastest.
Arguments:
- queries: bfloat16 [16384, 8, 128], P('ep', 'tp'), may hold values from -256 to 256
- keys: bfloat16 [16384, 4, 128], P('ep', 'tp'), may hold values from -8 to 8
- values: bfloat16 [16384, 4, 128], P('ep', 'tp'), may hold values from -6 to 6
- attn_lambda: float32 [8], P('tp'), may hold values from 0.3 to 0.8
- head_gain: float32 [128], replicated, may hold values from 0.1 to 1.9
- w_out: bfloat16 [1024, 2048], replicated, may hold values from -0.1875 to 0.1875
- moe_rows: bfloat16 [32768, 2048], P('ep'), may hold values from -6 to 6
- moe_gain: float32 [2048], replicated, may hold values from 0.1 to 1.9
- routes: int32 [32768, 2], P('ep'), may hold values from 0 to 63, all different within a row; in each aligned block of 128 rows (0 to 127, 128 to 255, ...) at most 8 rows name the same one
- route_weights: float32 [32768, 2], P('ep'), may hold values from 0.1 to 1
- w_gate: bfloat16 [64, 2048, 1024], P('ep', None, 'tp'), may hold values from -0.125 to 0.125
- w_up: bfloat16 [64, 2048, 1024], P('ep', None, 'tp'), may hold values from -0.125 to 0.125
- w_down: bfloat16 [64, 1024, 2048], P('ep', 'tp'), may hold values from -0.1875 to 0.1875
Outputs:
- mixer_out: bfloat16 [16384, 2048], P(('ep', 'tp'))
- moe_out: bfloat16 [32768, 2048], P(('ep', 'tp'))
Inputs may be any that keep to these rules, and one draw needn't show every extreme that they name: `routes`: each row names 2 different experts. In each aligned block of 128 rows (the rows of moe_out that one device holds) no expert is named by more than 8 rows, a bound that some block reaches.
All inputs are finite; a program needn't handle non-finite values.
Results may differ from a plain program's by a relative error of at most 0.011.
Values may be sent and summed in bfloat16 or wider, within the bound.
No kernel may reach another device: no remote copies, remote signals or barrier semaphores. Data moves between devices by JAX's collectives and lax.ppermute only.
A program may use at most 128 MiB of HBM per device.

v0:
```python
import jax
import jax.numpy as jnp
from jax import lax
from jax.sharding import PartitionSpec as P

EPSILON = 1e-06
MASKED = -1e30


def split_up(x, dim, size):
    before, after = (x.shape[:dim], x.shape[dim + 1 :])
    return jnp.moveaxis(x.reshape(*before, size, -1, *after), dim, 0)


def sum_at_owner(x, axis, dim):
    size = lax.axis_size(axis)
    tiles = lax.all_to_all(split_up(x, dim, size), axis, 0, 0, tiled=True)
    return jnp.sum(tiles.astype(jnp.float32), axis=0)


def joined_along(tiles, dim):
    tiles = jnp.moveaxis(tiles, 0, dim)
    lengths = tiles.shape
    return tiles.reshape(*lengths[:dim], lengths[dim] * lengths[dim + 1], *lengths[dim + 2 :])


def piecewise(x, axis, dim, work, out_dim):
    span = x.shape[dim]
    pieces = jnp.split(x, 2, axis=dim) if span % 2 == 0 else [x]
    first = jnp.arange(lax.axis_size(axis)) * span
    tiles = [lax.all_gather(section, axis) for section in pieces]
    made = [jax.vmap(work)(b, first + k * (span // len(pieces))) for k, b in enumerate(tiles)]
    return joined_along(jnp.concatenate(made, axis=out_dim + 1), out_dim)


def rms_scaled(values_f, gain):
    mean_sq = jnp.mean(values_f * values_f, axis=-1, keepdims=True)
    return values_f * lax.rsqrt(mean_sq + EPSILON) * gain


def slot_numbers(block_routes, experts):
    flat_ids = block_routes.reshape(-1)
    matches = (flat_ids[:, None] == lax.iota(jnp.int32, experts)[None, :]).astype(jnp.int32)
    earlier = jnp.cumsum(matches, axis=0) - matches
    return jnp.sum(earlier * matches, axis=1).reshape(block_routes.shape)


def fill_slots(block_rows, block_routes, experts, capacity):
    slot_ids = slot_numbers(block_routes, experts)
    model_width = block_rows.shape[1]
    copies = jnp.broadcast_to(block_rows[:, None, :], block_routes.shape + (model_width,))
    blank_slots = jnp.zeros((experts, capacity, model_width), block_rows.dtype)
    return (blank_slots.at[block_routes, slot_ids].set(copies), slot_ids)


def local(
    queries,
    keys,
    values,
    attn_lambda,
    head_gain,
    w_out,
    moe_rows,
    moe_gain,
    routes,
    route_weights,
    w_gate,
    w_up,
    w_down,
):
    positions = queries.shape[0]
    q_heads = queries.shape[1]
    kv_heads = keys.shape[1]
    head_dim = queries.shape[2] // 2
    value_dim = values.shape[2]
    per_key = q_heads // kv_heads
    first_pos = lax.axis_index("ep") * positions
    query_pos = first_pos + lax.iota(jnp.int32, positions)
    last_pos = first_pos + positions - 1
    query_view = queries.reshape(positions, kv_heads, per_key, 2, head_dim)
    inv_scale = head_dim ** (-0.5)
    start_max = jnp.full((positions, kv_heads, per_key, 2), MASKED, jnp.float32)
    start_total = jnp.zeros((positions, kv_heads, per_key, 2), jnp.float32)
    start_acc = jnp.zeros((positions, kv_heads, per_key, 2, value_dim), jnp.float32)
    carry = (start_max, start_total, start_acc)
    key_piece = lax.all_gather(keys, "ep", axis=0, tiled=True)
    value_piece = lax.all_gather(values, "ep", axis=0, tiled=True)
    shard_count = key_piece.shape[0] // positions
    together = 1
    for candidate in (2, 3, 4):
        if shard_count % candidate == 0:
            together = candidate
    block_len = together * positions
    blocks = shard_count // together
    key_blocks = key_piece.reshape(blocks, block_len, kv_heads, 2, head_dim)
    value_blocks = value_piece.reshape(blocks, block_len, kv_heads, value_dim)
    block_starts = block_len * lax.iota(jnp.int32, blocks)

    def visit(running, inputs):
        key_blk, value_blk, block_start = inputs

        def update(current):
            run_max, run_total, run_acc = current
            key_pos = block_start + lax.iota(jnp.int32, block_len)
            scores = (
                jnp.einsum(
                    "qkgmd,pkmd->qkgmp", query_view, key_blk, preferred_element_type=jnp.float32
                )
                * inv_scale
            )
            allowed = key_pos[None, :] <= query_pos[:, None]
            scores = jnp.where(allowed[:, None, None, None, :], scores, MASKED)
            new_max = jnp.maximum(run_max, jnp.max(scores, axis=-1))
            shrink = jnp.exp(run_max - new_max)
            weights = jnp.exp(scores - new_max[..., None])
            run_total = run_total * shrink + jnp.sum(weights, axis=-1)
            run_acc = run_acc * shrink[..., None] + jnp.einsum(
                "qkgmp,pkv->qkgmv",
                weights.astype(jnp.bfloat16),
                value_blk,
                preferred_element_type=jnp.float32,
            )
            return (new_max, run_total, run_acc)

        def keep(current):
            return current

        return (lax.cond(block_start <= last_pos, update, keep, running), None)

    carry, unused = lax.scan(visit, carry, (key_blocks, value_blocks, block_starts))
    run_max, run_total, run_acc = carry
    ratios = run_acc / run_total[..., None]
    lambda_view = attn_lambda.reshape(1, kv_heads, per_key, 1)
    head_out = ratios[:, :, :, 0] - lambda_view * ratios[:, :, :, 1]
    attn_rows = (
        rms_scaled(head_out, head_gain).astype(jnp.bfloat16).reshape(positions, q_heads * value_dim)
    )
    tp_count = lax.axis_size("tp")
    tp_id = lax.axis_index("tp")
    head_width = q_heads * value_dim
    w_local = lax.dynamic_slice_in_dim(w_out, tp_id * head_width, head_width, 0)
    mixer_out = sum_at_owner(
        jnp.dot(attn_rows, w_local, preferred_element_type=jnp.float32).astype(jnp.bfloat16),
        "tp",
        0,
    ).astype(jnp.bfloat16)
    experts = lax.axis_size("ep")
    dev_rows = moe_rows.shape[0] // tp_count
    top_count = routes.shape[1]
    capacity = max(2, 2 * dev_rows * top_count // experts)
    model_width = moe_rows.shape[1]
    hidden_units = w_gate.shape[2]
    own_routes = lax.dynamic_slice_in_dim(routes, tp_id * dev_rows, dev_rows, 0)
    own_weights = lax.dynamic_slice_in_dim(route_weights, tp_id * dev_rows, dev_rows, 0)

    def expert_hidden(slot_rows):
        flat_rows = slot_rows.reshape(-1, model_width)
        gate_out = jnp.dot(flat_rows, w_gate[0], preferred_element_type=jnp.float32)
        up_out = jnp.dot(flat_rows, w_up[0], preferred_element_type=jnp.float32)
        return (
            (jax.nn.silu(gate_out) * up_out)
            .astype(jnp.bfloat16)
            .reshape(slot_rows.shape[:-1] + (hidden_units,))
        )

    own_rows = rms_scaled(
        lax.dynamic_slice_in_dim(moe_rows, tp_id * dev_rows, dev_rows, 0).astype(jnp.float32),
        moe_gain,
    ).astype(jnp.bfloat16)
    outgoing, own_slots = fill_slots(own_rows, own_routes, experts, capacity)
    arrived = lax.all_to_all(outgoing, "ep", split_axis=0, concat_axis=0, tiled=True)

    def hidden_piece(slot_rows, begin_row):
        return expert_hidden(slot_rows)

    hidden = piecewise(arrived[None], "tp", 0, hidden_piece, 0)
    all_units = lax.all_to_all(hidden, "tp", split_axis=0, concat_axis=3, tiled=True)
    down_whole = lax.all_gather(w_down[0], "tp", axis=0, tiled=True)
    flat_units = all_units.reshape(-1, tp_count * hidden_units)
    summed_f = jnp.zeros((flat_units.shape[0], model_width), jnp.float32)
    for group in range(tp_count):
        unit_block = flat_units[:, group * hidden_units : (group + 1) * hidden_units]
        weight_block = down_whole[group * hidden_units : (group + 1) * hidden_units]
        group_part = jnp.dot(unit_block, weight_block, preferred_element_type=jnp.float32).astype(
            jnp.bfloat16
        )
        summed_f = summed_f + group_part.astype(jnp.float32)
    summed = summed_f.astype(jnp.bfloat16).reshape(all_units.shape[:-1] + (model_width,))
    returned = lax.all_to_all(summed, "ep", split_axis=1, concat_axis=1, tiled=True)[0]
    picked = returned[own_routes, own_slots]
    moe_out = jnp.sum(own_weights[..., None] * picked.astype(jnp.float32), axis=1).astype(
        jnp.bfloat16
    )
    return (mixer_out, moe_out)


def solution(mesh):
    return jax.shard_map(
        local,
        mesh=mesh,
        in_specs=(
            P("ep", "tp", None),
            P("ep", "tp", None),
            P("ep", "tp", None),
            P("tp"),
            P(),
            P(),
            P("ep", None),
            P(),
            P("ep", None),
            P("ep", None),
            P("ep", None, "tp"),
            P("ep", None, "tp"),
            P("ep", "tp", None),
        ),
        out_specs=(P(("ep", "tp"), None), P(("ep", "tp"), None)),
        check_vma=False,
    )
```

profile of v0, /device:TPU:2, one launch (start us, length us, event | category | flops | bytes accessed | tf_op | source)
XLA Modules:
  0.0 434.8 jit_solution(10305571413842020620)
XLA Ops:
  7.2 0.7 all-gather.7.cloned.1.call-update
  8.0 0.7 all-gather.9.cloned.1.call-update
  8.7 0.7 constant_dynamic-slice_fusion
  9.8 0.6 reduce-window.6
  11.1 1.2 fusion.25
  12.3 1.3 fusion.27
  13.6 0.6 broadcast_in_dim.57
  14.2 1.2 reshape.247
  15.7 33.0 %scatter_fusion = bf16[64,8,2048]{2,1,0:T(8,128)(2,1)S(1)} fusion(bf16[64,8,2048]{2,1,0:T(8,128)(2,1)S(1)} %broadcast_in_dim.36, s32[256]{0:T(256)S(1)} %reshape.245, bf16[256,2048]{1,0:T(8,128)(2,1)} %reshape.247), kind=kCustom, calls=%fused_computation.1 | custom fusion | bytes 3147776 | tf_op jit(solution)/shard_map/scatter | solution.py:53
  48.8 73.1 %all_to_all.30 = bf16[64,8,2048]{2,1,0:T(8,128)(2,1)} all-to-all(bf16[64,8,2048]{2,1,0:T(8,128)(2,1)S(1)} %scatter_fusion), channel_id=1, replica_groups=mesh['ep'=64,'tp'=4] {'ep'}, dimensions={0} | all-to-all | bytes 4194304 | tf_op jit(solution)/shard_map/all_to_all | solution.py:171
  122.7 14.7 %reshape.263 = bf16[16,1024,1,2,64]{4,3,1,0,2:T(2,128)(2,1)} reshape(bf16[16384,1,128]{2,0,1:T(8,128)(2,1)} %all-gather.7.cloned.1.call-done) | data formatting | bytes 8388608 | tf_op jit(solution)/shard_map/reshape | solution.py:95
  137.4 20.2 %copy.37 = bf16[16,1024,1,2,64]{1,4,3,2,0:T(8,128)(2,1)} copy(bf16[16,1024,1,2,64]{4,3,1,0,2:T(2,128)(2,1)} %reshape.263) | data formatting | bytes 8388608
  157.6 29.6 %all-gather.9.cloned.1.call-done = bf16[16384,1,128]{2,0,1:T(8,128)(2,1)} async-done(((bf16[256,1,128]{2,0,1:T(8,128)(2,1)}), bf16[16384,1,128]{2,0,1:T(8,128)(2,1)}) %all-gather.9.cloned.1.call-update) | async-done | bytes 4194320 | tf_op jit(solution)/shard_map/all_gather | solution.py:87
  187.2 6.4 %copy.39 = bf16[16,1024,1,128]{1,3,2,0:T(8,128)(2,1)} copy(bf16[16,1024,1,128]{3,1,0,2:T(8,128)(2,1)} %bitcast.160) | data formatting | bytes 8388608
  193.6 23.8 %while.15 = (s32[]{:T(128)}, f32[256,1,2,2]{0,2,3,1:T(2,128)S(1)}, f32[256,1,2,2]{0,2,3,1:T(2,128)S(1)}, f32[256,1,2,2,128]{0,4,3,2,1:T(8,128)S(1)}, s32[16]{0:T...) while((s32[]{:T(128)}, f32[256,1,2,2]{0,2,3,1:T(2,128)S(1)}, ...), condition=%wide.region_5.6_spmd.clone, body=%wide.region_0.5_spmd.clone.sunk | while | flops 411570432 | bytes 15156511 | solution.py:130
  193.7 0.6 dynamic_slice.56
  194.8 5.2 %conditional.3 = ((f32[256,1,2,2]{0,2,3,1:T(2,128)S(1)}, f32[256,1,2,2]{0,2,3,1:T(2,128)S(1)}, f32[256,1,2,2,128]{0,4,3,2,1:T(8,128)S(1)})) conditional(s32[]{:T(128)} %convert_element_type.131, (f32[256,1,2,2]{0,2,3,1:T(2,128)S(1)}, f32[256,1,2,2]{0,2,3,1:T(2,128)S(1)}, f32[256,1,2,2,128]{0,4,3,2,1:T(8,128)S(1)}) %tuple.48, (s32[]{:T(128)}, ...), branch_computations={%region_1.1_spmd, %region_2.4_spmd} | conditional | flops 411570432 | bytes 15155240 | solution.py:128
  195.6 1.8 fusion.4
  197.4 1.0 fusion.5
  198.5 1.5 fusion.11
  200.0 0.6 dynamic_slice.56
  201.2 0.6 dynamic_slice.56
  202.3 0.6 dynamic_slice.56
  203.5 0.6 dynamic_slice.56
  204.7 0.6 dynamic_slice.56
  207.0 0.6 dynamic_slice.56
  208.2 0.6 dynamic_slice.56
  217.5 55.6 %all-gather.11.cloned.1.call-done = bf16[256,8,2048]{2,1,0:T(8,128)(2,1)} async-done(((bf16[64,8,2048]{2,1,0:T(8,128)(2,1)}), bf16[256,8,2048]{2,1,0:T(8,128)(2,1)}) %all-gather.11.cloned.1.call-update) | async-done | bytes 8388624 | tf_op jit(solution)/shard_map/all_gather | solution.py:31
  273.1 5.9 %fusion.28 = f32[4,512,256]{2,1,0:T(8,128)S(1)} fusion(bf16[4,512,2048]{2,1,0:T(8,128)(2,1)} %bitcast.170, bf16[1,2048,256]{2,1,0:T(8,128)(2,1)S(1)} %copy-done), kind=kOutput, calls=%fused_computation.47 | convolution fusion | flops 2147483648 | bytes 11534336 | tf_op jit(solution)/shard_map/vmap()/dot_general | solution.py:159
  279.1 3.6 fusion.24
  282.7 4.0 all-to-all-start.2
  287.0 2.8 convolution_convert_fusion.4
  289.8 22.2 %all-to-all-done.2 = bf16[4,64,8,256]{3,2,1,0:T(8,128)(2,1)S(1)} async-done(((bf16[4,64,8,256]{3,2,1,0:T(8,128)(2,1)}), bf16[4,64,8,256]{3,2,1,0:T(8,128)(2,1)S(1)}, u32[]{:S(2)}, u32[]{:S(2)}) %all-to-all-start.2) | async-done | bytes 1048608 | tf_op jit(solution)/shard_map/all_to_all | solution.py:177
  312.0 3.7 all-to-all-start
  315.7 1.4 copy.65
  317.3 29.3 %all-gather.13.cloned.1.call-done = bf16[1,1024,2048]{2,1,0:T(8,128)(2,1)} async-done(((bf16[1,256,2048]{2,1,0:T(8,128)(2,1)}), bf16[1,1024,2048]{2,1,0:T(8,128)(2,1)}) %all-gather.13.cloned.1.call-update) | async-done | bytes 4194320 | tf_op jit(solution)/shard_map/all_gather | solution.py:178
  346.6 2.1 convolution_convert_fusion
  348.7 1.9 convolution_convert_fusion.1
  350.7 0.7 convolution_convert_fusion.2
  351.4 2.6 fusion.23
  354.0 1.0 copy-done.2
  355.0 10.6 %all-to-all-start.3 = ((bf16[1,64,8,2048]{3,2,0,1:T(8,128)(2,1)}), bf16[1,64,8,2048]{3,2,0,1:T(8,128)(2,1)S(1)}, u32[]{:S(2)}, u32[]{:S(2)}) async-start(bf16[1,64,8,2048]{3,2,0,1:T(8,128)(2,1)} %fusion.23), calls=%async_computation.3 | async-start | bytes 4194304 | tf_op jit(solution)/shard_map/all_to_all | solution.py:189
  365.7 0.7 constant_dynamic-slice_fusion.1
  366.5 2.2 reduce_sum.60
  368.7 48.1 %all-to-all-done.3 = bf16[1,64,8,2048]{3,2,0,1:T(8,128)(2,1)S(1)} async-done(((bf16[1,64,8,2048]{3,2,0,1:T(8,128)(2,1)}), bf16[1,64,8,2048]{3,2,0,1:T(8,128)(2,1)S(1)}, u32[]{:S(2)}, u32[]{:S(2)}) %all-to-all-start.3) | async-done | bytes 2097184 | tf_op jit(solution)/shard_map/all_to_all | solution.py:189
  416.8 5.2 %gather_fusion = bf16[256,2048]{1,0:T(8,128)(2,1)} fusion(bf16[64,8,2048]{2,1,0:T(8,128)(2,1)S(1)} %bitcast.159, s32[256]{0:T(256)S(1)} %reshape.239), kind=kCustom, calls=%fused_computation | custom fusion | bytes 2099200 | tf_op jit(solution)/shard_map/gather | solution.py:190
  422.0 2.4 reshape.258
  424.4 3.9 multiply_reduce_fusion
  (98 shorter events, 8.7 us)
Async XLA Ops:
  7.2 266.0 %copy-start = (bf16[1,2048,256]{2,1,0:T(8,128)(2,1)S(1)}, bf16[1,2048,256]{2,1,0:T(8,128)(2,1)}, u32[]{:S(2)}) copy-start(bf16[1,2048,256]{2,1,0:T(8,128)(2,1)} %param.28) | copy-start | bytes 3145732
  7.2 115.6 %all-gather.7.cloned.1.call-start = ((), (), s32[]{:S(2)}) async-start(), calls=%async_computation.4 | async-start | bytes 4259840 | tf_op jit(solution)/shard_map/all_gather | solution.py:86
  7.9 179.3 %all-gather.9.cloned.1.call-start = ((), (), s32[]{:S(2)}) async-start(), calls=%async_computation.5 | async-start | bytes 4259840 | tf_op jit(solution)/shard_map/all_gather | solution.py:87
  8.7 264.5 %all-gather.11.cloned.1.call-start = ((), (), s32[]{:S(2)}) async-start(), calls=%async_computation.6 | async-start | bytes 10485760 | tf_op jit(solution)/shard_map/all_gather | solution.py:31
  48.7 73.8 %copy-start.3 = (bf16[256,2,128]{2,1,0:T(2,128)(2,1)S(1)}, bf16[256,2,128]{2,1,0:T(2,128)(2,1)}, u32[]{:S(2)}) copy-start(bf16[256,2,128]{2,1,0:T(2,128)(2,1)} %param.17) | copy-start | bytes 393220
  48.7 73.9 %copy-start.4 = (f32[2]{0:T(128)S(1)}, f32[2]{0:T(128)}, u32[]{:S(2)}) copy-start(f32[2]{0:T(128)} %param.20) | copy-start | bytes 28
  48.8 73.9 %copy-start.5 = (f32[128]{0:T(128)S(1)}, f32[128]{0:T(128)}, u32[]{:S(2)}) copy-start(f32[128]{0:T(128)} %param.21) | copy-start | bytes 1540
  121.9 224.7 %all-gather.13.cloned.1.call-start = ((), (), s32[]{:S(2)}) async-start(), calls=%async_computation.7 | async-start | bytes 5242880 | tf_op jit(solution)/shard_map/all_gather | solution.py:178
  273.1 5.9 %copy-start.6 = (bf16[256,8,2048]{2,1,0:T(8,128)(2,1)S(1)}, bf16[256,8,2048]{2,1,0:T(8,128)(2,1)}, u32[]{:S(2)}) copy-start(bf16[256,8,2048]{2,1,0:T(8,128)(2,1)} %all-gather.11.cloned.1.call-done) | copy-start | bytes 25165828
  273.1 6.0 %copy-start.7 = (bf16[1,2048,256]{2,1,0:T(8,128)(2,1)S(1)}, bf16[1,2048,256]{2,1,0:T(8,128)(2,1)}, u32[]{:S(2)}) copy-start(bf16[1,2048,256]{2,1,0:T(8,128)(2,1)} %param.27) | copy-start | bytes 3145732
  282.7 29.3 %all-to-all-start.2 = ((bf16[4,64,8,256]{3,2,1,0:T(8,128)(2,1)}), bf16[4,64,8,256]{3,2,1,0:T(8,128)(2,1)S(1)}, u32[]{:S(2)}, u32[]{:S(2)}) async-start(bf16[4,64,8,256]{3,2,1,0:T(8,128)(2,1)} %fusion.24), calls=%async_computation.2 | async-start | bytes 2097152 | tf_op jit(solution)/shard_map/all_to_all | solution.py:177
  312.0 42.0 %all-to-all-start = ((bf16[4,64,2048]{2,1,0:T(8,128)(2,1)}), bf16[4,64,2048]{2,1,0:T(8,128)(2,1)S(1)}, u32[]{:S(2)}, u32[]{:S(2)}) async-start(bf16[4,64,2048]{2,1,0:T(8,128)(2,1)} %bitcast.26), calls=%async_computation | async-start | bytes 2097152 | tf_op jit(solution)/shard_map/all_to_all | solution.py:17
  346.6 4.0 copy-start.1
  354.0 1.0 copy-start.2
  355.0 61.8 %all-to-all-start.3 = ((bf16[1,64,8,2048]{3,2,0,1:T(8,128)(2,1)}), bf16[1,64,8,2048]{3,2,0,1:T(8,128)(2,1)S(1)}, u32[]{:S(2)}, u32[]{:S(2)}) async-start(bf16[1,64,8,2048]{3,2,0,1:T(8,128)(2,1)} %fusion.23), calls=%async_computation.3 | async-start | bytes 4194304 | tf_op jit(solution)/shard_map/all_to_all | solution.py:189
Sparse Core Ops, SparseCore 0:
  10.8 94.4 all-gather.6
  108.0 79.1 all-gather.8
  189.0 84.0 all-gather.10
  274.8 71.7 all-gather.12
where the time goes:
time: 438 us; the launch traced here: 435 us
  waiting for transfers between devices  187 us (43%)
  local copies, waits for them, and re-layouts  98.3 us (22%)
  blocking collectives  73.1 us (17%)
  matrix products  23 us (5%)
  starting transfers between devices  18.6 us (4%)
  between operations  14.1 us (3%)
  other arithmetic  11.5 us (3%)
  loops' own time  9.72 us (2%)
    all_to_all x1, blocking collectives, local(): lax.all_to_all(outgoing, 'ep', split_axis=0, concat_axis=0, tiled=True)  73.1 us
    all_gather x1, waiting for transfers between devices, piecewise(): tiles = [lax.all_gather(section, axis) for section in pieces]  55.6 us
    all_to_all x1, waiting for transfers between devices, local(): lax.all_to_all(summed, 'ep', split_axis=1, concat_axis=1, tiled=True)[0]  48.1 us
    scatter x1, local copies, waits for them, and re-layouts, fill_slots(): return (blank_slots.at[block_routes, slot_ids].set(copies), slot_ids)  33 us
    all_gather x1, waiting for transfers between devices, local(): value_piece = lax.all_gather(values, 'ep', axis=0, tiled=True)  29.6 us
    all_gather x1, waiting for transfers between devices, local(): down_whole = lax.all_gather(w_down[0], 'tp', axis=0, tiled=True)  29.3 us
    unnamed x22, local copies, waits for them, and re-layouts  28.1 us
    all_to_all x1, waiting for transfers between devices, local(): lax.all_to_all(hidden, 'tp', split_axis=0, concat_axis=3, tiled=True)  22.2 us
  transfers between devices with their start and end apart: 7, of which 5 were waited for; matrix products, arithmetic and copies ran while one was open for 28% of the time, Pallas kernels for 0%

commit v1 on v0

--- a/solution.py
+++ b/solution.py
@@ -84,7 +84,9 @@
     start_acc = jnp.zeros((positions, kv_heads, per_key, 2, value_dim), jnp.float32)
     carry = (start_max, start_total, start_acc)
     key_piece = lax.all_gather(keys, "ep", axis=0, tiled=True)
-    value_piece = lax.all_gather(values, "ep", axis=0, tiled=True)
+    value_piece = jnp.concatenate(
+        lax.all_to_all(jnp.stack([values] * lax.axis_size("ep")), "ep", 0, 0), axis=0
+    )
     shard_count = key_piece.shape[0] // positions
     together = 1
     for candidate in (2, 3, 4):

time: 438 us -> 457 us (1.043)
  starting transfers between devices: 18.6 us -> 98.9 us
  waiting for transfers between devices: 187 us -> 122 us
    all_to_all x1, starting transfers between devices: 10.6 us -> 84.6 us  [local(): lax.all_to_all(summed, 'ep', split_axis=1, concat_axis=1, tiled=True)[0]]
    all_to_all x0 -> x1, waiting for transfers between devices: none -> 60.2 us  [local(): lax.all_to_all(jnp.stack([values] * lax.axis_size('ep')), 'ep', 0, 0)]
    all_gather x1, waiting for transfers between devices: 55.6 us -> 0.02 us  [piecewise(): tiles = [lax.all_gather(section, axis) for section in pieces]]
    all_gather x1 -> x0, waiting for transfers between devices: 29.6 us -> none  [local(): value_piece = lax.all_gather(values, 'ep', axis=0, tiled=True)]
    all_gather x1, waiting for transfers between devices: 29.3 us -> 0.02 us  [local(): down_whole = lax.all_gather(w_down[0], 'tp', axis=0, tiled=True)]
    all_to_all x1, waiting for transfers between devices: 22.2 us -> 9.96 us  [local(): lax.all_to_all(hidden, 'tp', split_axis=0, concat_axis=3, tiled=True)]
    all_to_all x0 -> x1, starting transfers between devices: none -> 5.75 us  [local(): lax.all_to_all(jnp.stack([values] * lax.axis_size('ep')), 'ep', 0, 0)]
    unnamed x22 -> x24, local copies, waits for them, and re-layouts: 28.1 us -> 28.2 us
  transfers between devices with their start and end apart: 7 -> 7, of which waited for: 5 -> 4; matrix products, arithmetic and copies ran while one was open for 28% -> 27% of each run, Pallas kernels for 0% -> 0%
where the time goes in v1:
time: 457 us; the launch traced here: 454 us
  waiting for transfers between devices  122 us (27%)
  local copies, waits for them, and re-layouts  101 us (22%)
  starting transfers between devices  98.9 us (22%)
  blocking collectives  73.1 us (16%)
  matrix products  22.8 us (5%)
  between operations  14.1 us (3%)
  other arithmetic  11.5 us (3%)
  loops' own time  9.72 us (2%)
    all_to_all x1, starting transfers between devices, local(): lax.all_to_all(summed, 'ep', split_axis=1, concat_axis=1, tiled=True)[0]  84.6 us
    all_to_all x1, blocking collectives, local(): lax.all_to_all(outgoing, 'ep', split_axis=0, concat_axis=0, tiled=True)  73.1 us
    all_to_all x1, waiting for transfers between devices, local(): lax.all_to_all(jnp.stack([values] * lax.axis_size('ep')), 'ep', 0, 0)  60.2 us
    all_to_all x1, waiting for transfers between devices, local(): lax.all_to_all(summed, 'ep', split_axis=1, concat_axis=1, tiled=True)[0]  48.1 us
    scatter x1, local copies, waits for them, and re-layouts, fill_slots(): return (blank_slots.at[block_routes, slot_ids].set(copies), slot_ids)  33 us
    unnamed x24, local copies, waits for them, and re-layouts  28.2 us
    reshape x1, local copies, waits for them, and re-layouts, local(): key_blocks = key_piece.reshape(blocks, block_len, kv_heads, 2, head_dim)  14.8 us
    all_to_all x1, waiting for transfers between devices, local(): lax.all_to_all(hidden, 'tp', split_axis=0, concat_axis=3, tiled=True)  9.96 us
  transfers between devices with their start and end apart: 7, of which 4 were waited for; matrix products, arithmetic and copies ran while one was open for 27% of the time, Pallas kernels for 0%

profile of v1, /device:TPU:2, one launch (start us, length us, event | category | flops | bytes accessed | tf_op | source)
XLA Modules:
  0.0 453.6 jit_solution(12108201834496254006)
XLA Ops:
  7.2 0.7 all-gather.6.cloned.1.call-update
  8.0 0.7 constant_dynamic-slice_fusion
  9.1 0.6 reduce-window.6
  10.4 1.2 fusion.25
  11.6 1.3 fusion.27
  12.9 0.6 broadcast_in_dim.57
  13.5 1.2 reshape.246
  15.0 33.0 %scatter_fusion = bf16[64,8,2048]{2,1,0:T(8,128)(2,1)S(1)} fusion(bf16[64,8,2048]{2,1,0:T(8,128)(2,1)S(1)} %broadcast_in_dim.36, s32[256]{0:T(256)S(1)} %reshape.244, bf16[256,2048]{1,0:T(8,128)(2,1)} %reshape.246), kind=kCustom, calls=%fused_computation.1 | custom fusion | bytes 3147776 | tf_op jit(solution)/shard_map/scatter | solution.py:53
  48.0 73.1 %all_to_all.35 = bf16[64,8,2048]{2,1,0:T(8,128)(2,1)} all-to-all(bf16[64,8,2048]{2,1,0:T(8,128)(2,1)S(1)} %scatter_fusion), channel_id=1, replica_groups=mesh['ep'=64,'tp'=4] {'ep'}, dimensions={0} | all-to-all | bytes 4194304 | tf_op jit(solution)/shard_map/all_to_all | solution.py:173
  121.1 3.0 stack.2
  124.1 5.8 %all-to-all-start = ((bf16[64,256,1,128]{3,1,2,0:T(8,128)(2,1)}), bf16[64,256,1,128]{3,1,2,0:T(8,128)(2,1)}, u32[]{:S(2)}, u32[]{:S(2)}) async-start(bf16[64,256,1,128]{3,1,2,0:T(8,128)(2,1)} %stack.2), calls=%async_computation | async-start | bytes 8388608 | tf_op jit(solution)/shard_map/all_to_all | solution.py:88
  130.9 14.8 %reshape.262 = bf16[16,1024,1,2,64]{4,3,1,0,2:T(2,128)(2,1)} reshape(bf16[16384,1,128]{2,0,1:T(8,128)(2,1)} %all-gather.6.cloned.1.call-done) | data formatting | bytes 8388608 | tf_op jit(solution)/shard_map/reshape | solution.py:97
  145.6 20.2 %copy.37 = bf16[16,1024,1,2,64]{1,4,3,2,0:T(8,128)(2,1)} copy(bf16[16,1024,1,2,64]{4,3,1,0,2:T(2,128)(2,1)} %reshape.262) | data formatting | bytes 8388608
  165.8 60.2 %all-to-all-done = bf16[64,256,1,128]{3,1,2,0:T(8,128)(2,1)} async-done(((bf16[64,256,1,128]{3,1,2,0:T(8,128)(2,1)}), bf16[64,256,1,128]{3,1,2,0:T(8,128)(2,1)}, u32[]{:S(2)}, u32[]{:S(2)}) %all-to-all-start) | async-done | bytes 4194336 | tf_op jit(solution)/shard_map/all_to_all | solution.py:88
  226.0 6.4 %copy.39 = bf16[16,1024,1,128]{1,3,2,0:T(8,128)(2,1)} copy(bf16[16,1024,1,128]{3,1,0,2:T(8,128)(2,1)} %bitcast.18) | data formatting | bytes 8388608
  232.5 23.8 %while.15 = (s32[]{:T(128)}, f32[256,1,2,2]{0,2,3,1:T(2,128)S(1)}, f32[256,1,2,2]{0,2,3,1:T(2,128)S(1)}, f32[256,1,2,2,128]{0,4,3,2,1:T(8,128)S(1)}, s32[16]{0:T...) while((s32[]{:T(128)}, f32[256,1,2,2]{0,2,3,1:T(2,128)S(1)}, ...), condition=%wide.region_5.6_spmd.clone, body=%wide.region_0.5_spmd.clone.sunk | while | flops 411570432 | bytes 15156511 | solution.py:132
  233.6 5.2 %conditional.3 = ((f32[256,1,2,2]{0,2,3,1:T(2,128)S(1)}, f32[256,1,2,2]{0,2,3,1:T(2,128)S(1)}, f32[256,1,2,2,128]{0,4,3,2,1:T(8,128)S(1)})) conditional(s32[]{:T(128)} %convert_element_type.131, (f32[256,1,2,2]{0,2,3,1:T(2,128)S(1)}, f32[256,1,2,2]{0,2,3,1:T(2,128)S(1)}, f32[256,1,2,2,128]{0,4,3,2,1:T(8,128)S(1)}) %tuple.48, (s32[]{:T(128)}, ...), branch_computations={%region_1.1_spmd, %region_2.4_spmd} | conditional | flops 411570432 | bytes 15155240 | solution.py:130
  234.4 1.8 fusion.4
  236.3 1.0 fusion.5
  237.3 1.5 fusion.11
  240.0 0.6 dynamic_slice.56
  243.5 0.6 dynamic_slice.56
  244.6 0.6 dynamic_slice.56
  245.8 0.6 dynamic_slice.56
  248.1 0.6 dynamic_slice.56
  249.3 0.6 dynamic_slice.56
  250.4 0.6 dynamic_slice.56
  252.8 0.6 dynamic_slice.56
  256.4 5.9 %fusion.28 = f32[4,512,256]{2,1,0:T(8,128)S(1)} fusion(bf16[4,512,2048]{2,1,0:T(8,128)(2,1)} %bitcast.171, bf16[1,2048,256]{2,1,0:T(8,128)(2,1)S(1)} %copy-done), kind=kOutput, calls=%fused_computation.47 | convolution fusion | flops 2147483648 | bytes 11534336 | tf_op jit(solution)/shard_map/vmap()/dot_general | solution.py:161
  262.3 3.6 fusion.24
  266.0 4.5 all-to-all-start.3
  270.7 2.7 convolution_convert_fusion.4
  273.4 10.0 %all-to-all-done.3 = bf16[4,64,8,256]{3,2,1,0:T(8,128)(2,1)S(1)} async-done(((bf16[4,64,8,256]{3,2,1,0:T(8,128)(2,1)}), bf16[4,64,8,256]{3,2,1,0:T(8,128)(2,1)S(1)}, u32[]{:S(2)}, u32[]{:S(2)}) %all-to-all-start.3) | async-done | bytes 1048608 | tf_op jit(solution)/shard_map/all_to_all | solution.py:179
  283.4 3.7 all-to-all-start.1
  287.1 1.4 copy.65
  288.8 2.1 convolution_convert_fusion
  290.9 1.9 convolution_convert_fusion.1
  292.8 0.7 convolution_convert_fusion.2
  293.5 2.6 fusion.23
  296.1 2.6 all-to-all-done.1
  298.7 1.0 copy-done.2
  299.7 84.6 %all-to-all-start.4 = ((bf16[1,64,8,2048]{3,2,0,1:T(8,128)(2,1)}), bf16[1,64,8,2048]{3,2,0,1:T(8,128)(2,1)S(1)}, u32[]{:S(2)}, u32[]{:S(2)}) async-start(bf16[1,64,8,2048]{3,2,0,1:T(8,128)(2,1)} %fusion.23), calls=%async_computation.4 | async-start | bytes 4194304 | tf_op jit(solution)/shard_map/all_to_all | solution.py:191
  384.5 0.7 constant_dynamic-slice_fusion.1
  385.3 2.2 reduce_sum.60
  387.5 48.1 %all-to-all-done.4 = bf16[1,64,8,2048]{3,2,0,1:T(8,128)(2,1)S(1)} async-done(((bf16[1,64,8,2048]{3,2,0,1:T(8,128)(2,1)}), bf16[1,64,8,2048]{3,2,0,1:T(8,128)(2,1)S(1)}, u32[]{:S(2)}, u32[]{:S(2)}) %all-to-all-start.4) | async-done | bytes 2097184 | tf_op jit(solution)/shard_map/all_to_all | solution.py:191
  435.6 5.2 %gather_fusion = bf16[256,2048]{1,0:T(8,128)(2,1)} fusion(bf16[64,8,2048]{2,1,0:T(8,128)(2,1)S(1)} %bitcast.160, s32[256]{0:T(256)S(1)} %reshape.238), kind=kCustom, calls=%fused_computation | custom fusion | bytes 2099200 | tf_op jit(solution)/shard_map/gather | solution.py:192
  440.8 2.4 reshape.257
  443.2 3.9 multiply_reduce_fusion
  (100 shorter events, 8.9 us)
Async XLA Ops:
  7.2 249.2 %copy-start = (bf16[1,2048,256]{2,1,0:T(8,128)(2,1)S(1)}, bf16[1,2048,256]{2,1,0:T(8,128)(2,1)}, u32[]{:S(2)}) copy-start(bf16[1,2048,256]{2,1,0:T(8,128)(2,1)} %param.28) | copy-start | bytes 3145732
  7.2 123.7 %all-gather.6.cloned.1.call-start = ((), (), s32[]{:S(2)}) async-start(), calls=%async_computation.5 | async-start | bytes 4259840 | tf_op jit(solution)/shard_map/all_gather | solution.py:86
  7.9 248.4 %all-gather.8.cloned.1.call-start = ((), (), s32[]{:S(2)}) async-start(), calls=%async_computation.6 | async-start | bytes 10485760 | tf_op jit(solution)/shard_map/all_gather | solution.py:31
  48.0 73.1 %copy-start.4 = (bf16[256,1,128]{2,0,1:T(8,128)(2,1)S(1)}, bf16[256,1,128]{2,0,1:T(8,128)(2,1)}, u32[]{:S(2)}) copy-start(bf16[256,1,128]{2,0,1:T(8,128)(2,1)} %param.19) | copy-start | bytes 196612
  124.1 6.5 %copy-start.3 = (bf16[256,2,128]{2,1,0:T(2,128)(2,1)S(1)}, bf16[256,2,128]{2,1,0:T(2,128)(2,1)}, u32[]{:S(2)}) copy-start(bf16[256,2,128]{2,1,0:T(2,128)(2,1)} %param.17) | copy-start | bytes 393220
  124.1 6.7 %copy-start.5 = (f32[2]{0:T(128)S(1)}, f32[2]{0:T(128)}, u32[]{:S(2)}) copy-start(f32[2]{0:T(128)} %param.20) | copy-start | bytes 28
  124.1 6.7 %copy-start.6 = (f32[128]{0:T(128)S(1)}, f32[128]{0:T(128)}, u32[]{:S(2)}) copy-start(f32[128]{0:T(128)} %param.21) | copy-start | bytes 1540
  124.1 101.9 %all-to-all-start = ((bf16[64,256,1,128]{3,1,2,0:T(8,128)(2,1)}), bf16[64,256,1,128]{3,1,2,0:T(8,128)(2,1)}, u32[]{:S(2)}, u32[]{:S(2)}) async-start(bf16[64,256,1,128]{3,1,2,0:T(8,128)(2,1)} %stack.2), calls=%async_computation | async-start | bytes 8388608 | tf_op jit(solution)/shard_map/all_to_all | solution.py:88
  129.9 158.9 %all-gather.10.cloned.1.call-start = ((), (), s32[]{:S(2)}) async-start(), calls=%async_computation.7 | async-start | bytes 5242880 | tf_op jit(solution)/shard_map/all_gather | solution.py:180
  256.3 5.9 %copy-start.7 = (bf16[256,8,2048]{2,1,0:T(8,128)(2,1)S(1)}, bf16[256,8,2048]{2,1,0:T(8,128)(2,1)}, u32[]{:S(2)}) copy-start(bf16[256,8,2048]{2,1,0:T(8,128)(2,1)} %all-gather.8.cloned.1.call-done) | copy-start | bytes 25165828
  256.4 6.0 %copy-start.8 = (bf16[1,2048,256]{2,1,0:T(8,128)(2,1)S(1)}, bf16[1,2048,256]{2,1,0:T(8,128)(2,1)}, u32[]{:S(2)}) copy-start(bf16[1,2048,256]{2,1,0:T(8,128)(2,1)} %param.27) | copy-start | bytes 3145732
  266.0 17.4 %all-to-all-start.3 = ((bf16[4,64,8,256]{3,2,1,0:T(8,128)(2,1)}), bf16[4,64,8,256]{3,2,1,0:T(8,128)(2,1)S(1)}, u32[]{:S(2)}, u32[]{:S(2)}) async-start(bf16[4,64,8,256]{3,2,1,0:T(8,128)(2,1)} %fusion.24), calls=%async_computation.3 | async-start | bytes 2097152 | tf_op jit(solution)/shard_map/all_to_all | solution.py:179
  283.4 15.3 %all-to-all-start.1 = ((bf16[4,64,2048]{2,1,0:T(8,128)(2,1)}), bf16[4,64,2048]{2,1,0:T(8,128)(2,1)S(1)}, u32[]{:S(2)}, u32[]{:S(2)}) async-start(bf16[4,64,2048]{2,1,0:T(8,128)(2,1)} %bitcast.27), calls=%async_computation.1 | async-start | bytes 2097152 | tf_op jit(solution)/shard_map/all_to_all | solution.py:17
  288.8 4.1 copy-start.1
  298.7 1.0 copy-start.2
  299.7 135.9 %all-to-all-start.4 = ((bf16[1,64,8,2048]{3,2,0,1:T(8,128)(2,1)}), bf16[1,64,8,2048]{3,2,0,1:T(8,128)(2,1)S(1)}, u32[]{:S(2)}, u32[]{:S(2)}) async-start(bf16[1,64,8,2048]{3,2,0,1:T(8,128)(2,1)} %fusion.23), calls=%async_computation.4 | async-start | bytes 4194304 | tf_op jit(solution)/shard_map/all_to_all | solution.py:191
Sparse Core Ops, SparseCore 0:
  10.8 94.4 all-gather.5
  121.2 82.0 all-gather.7
  205.1 51.7 all-gather.9
